TPU v7x, 256 devices: a whole 4x4x8 slice. The times are simulated.
256 devices in a mesh: row: 32 (over z, y), col: 8 (over x, core).
Axes of the slice: x: 4, y: 4, z: 8, core: 2. Of those that a mesh axis runs over, the one named last changes fastest.
Arguments:
- tokens: bfloat16 [2, 65536, 1024], P(None, 'row'), may hold values from -6 to 6
- norm_gain: float32 [1024], replicated, may hold values from 0.1 to 1.9
- w_fourier_in: bfloat16 [1024, 512], P(None, 'col'), may hold values from -0.1875 to 0.1875
- w_gate: bfloat16 [1024, 1024], replicated, may hold values from -0.1875 to 0.1875
- w_spectrum: bfloat16 [512, 1024], replicated, may hold values from -0.25 to 0.25
- w_output: bfloat16 [1024, 1024], P(None, 'col'), may hold values from -0.375 to 0.375
Outputs:
- block_output: bfloat16 [2, 65536, 1024], P(None, 'row', 'col')
All inputs are finite; a program needn't handle non-finite values.
Results may differ from a plain program's by a relative error of at most 0.015.
Values may be sent and summed in bfloat16 or wider, within the bound.
A program may use at most 320 MiB of HBM per device.

v0:
```python
import functools

import jax
import jax.numpy as jnp
import numpy as np
from jax import lax
from jax.experimental import pallas as pl
from jax.experimental.pallas import tpu as pltpu
from jax.sharding import PartitionSpec as P

GROUP_WIDTH = 64
FIRST_LEN = 256


norm_eps = 1e-06


def shortened(value):
    return jax.tree.map(lambda a: a.astype(jnp.bfloat16) if a.dtype == jnp.float32 else a, value)


def over_all(value, axis, dim, absorb, carry):
    whole = jax.tree.map(lambda part: lax.all_gather(part, axis, axis=dim, tiled=True), value)
    return absorb(carry, whole, jnp.int32(0))


def dft_tables(length_in, length_out, period):
    left_index = lax.broadcasted_iota(jnp.int32, (length_in, length_out), 0)
    right_index = lax.broadcasted_iota(jnp.int32, (length_in, length_out), 1)
    angles = (left_index * right_index % period).astype(jnp.float32) * (2.0 * jnp.pi / period)
    return (jnp.cos(angles), jnp.sin(angles))


def transform_first(cube, table):
    return jnp.einsum("cpq,pk->ckq", cube, table, precision=lax.Precision.HIGHEST)


def transform_second(cube, table):
    return jnp.einsum("ckq,qj->cjk", cube, table, precision=lax.Precision.HIGHEST)


def positional(real_part, imag_part):
    rows_count, seq_total = real_part.shape
    second_len = seq_total // FIRST_LEN
    cos_first, sin_first = dft_tables(FIRST_LEN, FIRST_LEN, FIRST_LEN)
    cos_twist, sin_twist = dft_tables(FIRST_LEN, second_len, seq_total)
    cos_second, sin_second = dft_tables(second_len, second_len, second_len)
    real_cube = real_part.reshape(rows_count, FIRST_LEN, second_len)
    imag_cube = imag_part.reshape(rows_count, FIRST_LEN, second_len)
    section_real = transform_first(real_cube, cos_first) + transform_first(imag_cube, sin_first)
    section_imag = transform_first(imag_cube, cos_first) - transform_first(real_cube, sin_first)
    twist_real = section_real * cos_twist + section_imag * sin_twist
    twist_imag = section_imag * cos_twist - section_real * sin_twist
    summed = transform_second(twist_real, cos_second) + transform_second(twist_imag, sin_second)
    norm_scale = 1.0 / jnp.sqrt(jnp.float32(seq_total * GROUP_WIDTH))
    return (summed.reshape(rows_count, seq_total) * norm_scale).astype(jnp.bfloat16)


def on_device(tokens, norm_gain, w_fourier_in, w_gate, w_spectrum, w_output):
    batches, seq_local, features = tokens.shape
    tokens_count = batches * seq_local
    widened = tokens.astype(jnp.float32)
    inverse = lax.rsqrt(jnp.mean(widened * widened, axis=-1, keepdims=True) + norm_eps)
    normed = (widened * inverse * norm_gain).astype(jnp.bfloat16).reshape(tokens_count, features)
    fourier_in = jnp.dot(normed, w_fourier_in, preferred_element_type=jnp.float32).astype(
        jnp.bfloat16
    )
    local_groups = w_fourier_in.shape[1] // GROUP_WIDTH
    grouped = fourier_in.astype(jnp.float32).reshape(batches, seq_local, local_groups, GROUP_WIDTH)
    cos_group, sin_group = dft_tables(GROUP_WIDTH, GROUP_WIDTH, GROUP_WIDTH)
    real_part = jnp.einsum(
        "btgn,nm->bgmt", grouped, cos_group, precision=lax.Precision.HIGHEST
    ).reshape(-1, seq_local)
    imag_part = -jnp.einsum(
        "btgn,nm->bgmt", grouped, sin_group, precision=lax.Precision.HIGHEST
    ).reshape(-1, seq_local)
    real_part = lax.all_to_all(
        shortened(real_part), "row", split_axis=0, concat_axis=1, tiled=True
    ).astype(real_part.dtype)
    imag_part = lax.all_to_all(
        shortened(imag_part), "row", split_axis=0, concat_axis=1, tiled=True
    ).astype(imag_part.dtype)
    spectrum = positional(real_part, imag_part)
    spectrum = lax.all_to_all(spectrum, "row", split_axis=1, concat_axis=0, tiled=True)
    spectrum = spectrum.reshape(batches, local_groups * GROUP_WIDTH, seq_local)
    spectrum = jnp.transpose(spectrum, (0, 2, 1)).reshape(tokens_count, local_groups * GROUP_WIDTH)

    def add_spectrum(running, portion, beginning):
        weight_rows = lax.dynamic_slice_in_dim(w_spectrum, beginning, portion.shape[1], 0)
        return running + jnp.dot(portion, weight_rows, preferred_element_type=jnp.float32)

    mixed_pre = over_all(
        spectrum, "col", 1, add_spectrum, jnp.zeros((tokens_count, features), jnp.float32)
    ).astype(jnp.bfloat16)
    gate_pre = jnp.dot(normed, w_gate, preferred_element_type=jnp.float32)
    mixed = (jax.nn.sigmoid(gate_pre) * mixed_pre.astype(jnp.float32)).astype(jnp.bfloat16)
    result = jnp.dot(mixed, w_output, preferred_element_type=jnp.float32)
    return result.astype(jnp.bfloat16).reshape(batches, seq_local, -1)


MESH = pl.DeviceIdType.MESH
HALF = GROUP_WIDTH // 2


def channel_tables():
    n = np.arange(GROUP_WIDTH)
    fold = np.zeros((GROUP_WIDTH, GROUP_WIDTH))
    unfold = np.zeros((GROUP_WIDTH, GROUP_WIDTH))
    for d in range(GROUP_WIDTH):
        if d <= HALF:
            fold[:, d] = np.cos(2 * np.pi * (n * d % GROUP_WIDTH) / GROUP_WIDTH)
            unfold[d, d] = 1.0
            unfold[d, (GROUP_WIDTH - d) % GROUP_WIDTH] = 1.0
        else:
            m = d - HALF
            fold[:, d] = np.sin(2 * np.pi * (n * m % GROUP_WIDTH) / GROUP_WIDTH)
            unfold[d, m] = -1.0
            unfold[d, GROUP_WIDTH - m] = 1.0
    return fold, unfold


def position_tables(n):
    a = np.arange(n)
    ang = 2 * np.pi * (np.outer(a, a) % n) / n
    first = np.concatenate([np.cos(ang), np.sin(ang)], 0)
    second = np.concatenate([np.cos(ang), np.sin(ang)], 1)
    phi = 2 * np.pi * np.outer(a, a) / (n * n)
    scale = 1.0 / np.sqrt(n * n * GROUP_WIDTH)
    c, s = np.cos(phi) * scale, np.sin(phi) * scale
    twist = np.stack([np.stack([c, s]), np.stack([s, -c])])
    return first, second, twist


def mixer_kernel(
    rows, cols, tok, gain, wf, wg, wspec, wout, fold, unfold, f1, f2, tw, out,
    tokv, wgv, wsv, ws, wo, wp, gate, inv, ysc, osc, s1, x1, s2, spec,
    tsem, wsem, s1s, s1r, s2s, spr, fws,
):
    batches, seq_local, features = tok.shape
    cpd, steps, n = x1.shape[2:]
    me = lax.axis_index("row")
    col = lax.axis_index("col")
    sib = col + 1 - 2 * lax.rem(col, 2)
    chips = cols // 2
    chunk = 4 * n
    chunks = seq_local // chunk

    def peer(i):
        return lax.rem(me + i, rows)

    def xpeer(j):
        return lax.rem(col + 2 * j, cols)

    loads = {}
    for b in range(batches):
        for j in range(chunks):
            part = pl.ds(j * chunk, chunk)
            loads[b, j] = pltpu.make_async_copy(
                tok.at[b, part], tokv.at[b, part], tsem.at[b, j]
            )
            loads[b, j].start()
    wload = pltpu.make_async_copy(wg, wgv, wsem.at[0])
    wload.start()
    sload = pltpu.make_async_copy(wspec, wsv, wsem.at[1])
    sload.start()
    oload = pltpu.make_async_copy(wout, wo, wsem.at[2])
    oload.start()

    barrier = pltpu.get_barrier_semaphore()
    for i in range(1, rows):
        pl.semaphore_signal(barrier, inc=1, device_id={"row": peer(i)}, device_id_type=MESH)
    for j in range(1, chips):
        pl.semaphore_signal(barrier, inc=1, device_id={"col": xpeer(j)}, device_id_type=MESH)
    pl.semaphore_signal(barrier, inc=1, device_id={"col": sib}, device_id_type=MESH)

    gained = []
    lanes = 128
    for k in range(features // lanes):
        column = jnp.broadcast_to(gain[:, k * lanes:(k + 1) * lanes], (lanes, lanes)).T
        gained.append(column)
        w = wf[k * lanes:(k + 1) * lanes, :].astype(jnp.float32) * column[:, :1]
        wp[k * lanes:(k + 1) * lanes, :] = jnp.dot(
            w, fold[...], precision=lax.Precision.HIGHEST, preferred_element_type=jnp.float32
        ).astype(jnp.bfloat16)

    def project(b):
        for j in range(chunks):
            loads[b, j].wait()
            t = tokv[b, j * chunk:(j + 1) * chunk, :]
            w = t.astype(jnp.float32)
            scale = lax.rsqrt(jnp.mean(w * w, axis=-1, keepdims=True) + norm_eps)
            inv[b, j * chunk:(j + 1) * chunk, :] = scale
            y = jnp.dot(t, wp[...], preferred_element_type=jnp.float32) * scale
            for k in range(4):
                ysc[:, 4 * j + k, :] = y[k * n:(k + 1) * n, :].T
        s1[b] = ysc[...].astype(jnp.bfloat16)

    def first_copy(b, i, src):
        to = peer(i)
        return pltpu.make_async_remote_copy(
            src_ref=s1.at[b, pl.ds(to * cpd, cpd)],
            dst_ref=x1.at[b, src],
            send_sem=s1s.at[b, i],
            recv_sem=s1r.at[b, src],
            device_id={"row": to},
            device_id_type=MESH,
        )

    def send_first(b):
        for i in ORDER(rows):
            first_copy(b, i, me).start()
        x1[b, me] = s1[b, pl.ds(me * cpd, cpd)]

    def wait_first(b):
        for i in range(1, rows):
            first_copy(b, i, peer(i)).wait_recv()

    def gates(b, j):
        part = slice(j * chunk, (j + 1) * chunk)
        g = jnp.dot(tokv[b, part, :], wgv[...], preferred_element_type=jnp.float32)
        half = 0.5 * inv[b, part, :]
        gate[b, part, :] = (0.5 * jnp.tanh(g * half) + 0.5).astype(jnp.bfloat16)

    def transform(b):
        for c in range(cpd):
            kind = (lax.rem(me * cpd + c, GROUP_WIDTH) > HALF).astype(jnp.int32)
            x = x1[b, :, c].reshape(n, n)
            g = jnp.dot(f1[...], x, preferred_element_type=jnp.float32)
            ca, sa = tw[kind, 0], tw[kind, 1]
            u = g[:n] * ca - g[n:] * sa
            v = -(g[:n] * sa + g[n:] * ca)
            t = jnp.concatenate([u.astype(jnp.bfloat16), v.astype(jnp.bfloat16)], axis=1)
            o = lax.dot_general(
                f2[...], t, (((1,), (1,)), ((), ())), preferred_element_type=jnp.float32
            )
            osc[:, c, :] = o
        s2[b] = osc[...].astype(jnp.bfloat16)

    def second_copy(b, i, src):
        to = peer(i)
        return pltpu.make_async_remote_copy(
            src_ref=s2.at[b, pl.ds(to * steps, steps)],
            dst_ref=spec.at[col, b, src],
            send_sem=s2s.at[b, i],
            recv_sem=spr.at[col, b, src],
            device_id={"row": to},
            device_id_type=MESH,
        )

    def send_second(b):
        for i in ORDER(rows):
            second_copy(b, i, me).start()
        spec[col, b, me] = s2[b, pl.ds(me * steps, steps)]

    def share(b, src, owner, slot, to):
        return pltpu.make_async_remote_copy(
            src_ref=spec.at[owner, b, src],
            dst_ref=spec.at[owner, b, src],
            send_sem=fws.at[slot, b, src],
            recv_sem=spr.at[owner, b, src],
            device_id={"col": to},
            device_id_type=MESH,
        )

    def relay_own(b, i):
        src = peer(i)
        if i > 0:
            second_copy(b, i, src).wait_recv()
        for j in range(1, chips):
            share(b, src, col, j - 1, xpeer(j)).start()
        share(b, src, col, chips - 1, sib).start()

    def relay_far(b, i):
        src = peer(i)
        for j in range(1, chips):
            share(b, src, xpeer(j), chips - 1 + j, sib).wait_recv()
            share(b, src, xpeer(j), chips - 1 + j, sib).start()

    def relay_order():
        return [0] + list(RECV(rows))

    def relay(b, i):
        order = relay_order()
        relay_own(b, order[i])
        if i > 1:
            relay_far(b, order[i - 2])

    def relay_tail(b):
        order = relay_order()
        for i in order[-2:]:
            relay_far(b, i)
        for i in order:
            src = peer(i)
            share(b, src, sib, 0, sib).wait_recv()
            for j in range(1, chips):
                share(b, src, lax.rem(sib + 2 * j, cols), 0, sib).wait_recv()

    def finish(b, j):
        part = slice(j * chunk, (j + 1) * chunk)
        pieces = []
        for k in range(4):
            piece = spec[:, b, :, 4 * j + k].reshape(cols * rows * cpd, n)
            pieces.append(piece.T)
        lhs = jnp.concatenate(pieces, axis=0)
        pre = jnp.dot(lhs, ws[...], preferred_element_type=jnp.float32)
        mixed = (gate[b, part, :].astype(jnp.float32) * pre).astype(jnp.bfloat16)
        out[b, part, :] = jnp.dot(
            mixed, wo[...], preferred_element_type=jnp.float32
        ).astype(jnp.bfloat16)

    project(0)
    pl.semaphore_wait(barrier, rows - 1 + chips)
    send_first(0)
    for b in range(1, batches):
        project(b)
        send_first(b)
    wload.wait()
    for k in range(features // lanes):
        part = slice(k * lanes, (k + 1) * lanes)
        scaled = wgv[part, :].astype(jnp.float32) * gained[k][:, :1]
        wgv[part, :] = scaled.astype(jnp.bfloat16)
    for j in range(chunks):
        gates(0, j)
    sload.wait()
    for k in range(wsv.shape[0] // GROUP_WIDTH):
        part = slice(k * GROUP_WIDTH, (k + 1) * GROUP_WIDTH)
        ws[part, :] = jnp.dot(
            unfold[...], wsv[part, :], preferred_element_type=jnp.float32
        ).astype(jnp.bfloat16)
    oload.wait()
    for b in range(batches):
        wait_first(b)
        transform(b)
        send_second(b)
        if b + 1 < batches:
            for j in range(chunks):
                gates(b + 1, j)
    for i in range(rows):
        relay(0, i)
    relay_tail(0)
    for b in range(batches):
        for j in range(chunks):
            finish(b, j)
            if b + 1 < batches:
                for i in range(j * rows // chunks, (j + 1) * rows // chunks):
                    relay(b + 1, i)
        if b + 1 < batches:
            relay_tail(b + 1)
    for b in range(batches):
        for i in range(1, rows):
            first_copy(b, i, me).wait_send()
            second_copy(b, i, me).wait_send()
        for i in range(rows):
            for slot in range(2 * chips - 1):
                share(b, peer(i), col, slot, sib).wait_send()


def ORDER(rows):
    return range(1, rows)


def RECV(rows):
    return range(rows - 1, 0, -1)


def fused(rows, cols, tokens, norm_gain, w_fourier_in, w_gate, w_spectrum, w_output):
    batches, seq_local, features = tokens.shape
    n = int(round((seq_local * rows) ** 0.5))
    channels = w_fourier_in.shape[1]
    cpd = channels // rows
    steps = seq_local // n
    fold, unfold = channel_tables()
    first, second, twist = position_tables(n)
    local_groups = channels // GROUP_WIDTH
    vmem = pl.BlockSpec(memory_space=pltpu.VMEM)
    hbm = pl.BlockSpec(memory_space=pl.ANY)
    chunks = seq_local // (4 * n)
    dma = pltpu.SemaphoreType.DMA
    return pl.pallas_call(
        functools.partial(mixer_kernel, rows, cols),
        out_shape=jax.ShapeDtypeStruct((batches, seq_local, w_output.shape[1]), jnp.bfloat16),
        in_specs=[hbm, vmem, vmem, hbm, hbm, hbm, vmem, vmem, vmem, vmem, vmem],
        out_specs=vmem,
        scratch_shapes=[
            pltpu.VMEM(tokens.shape, jnp.bfloat16),
            pltpu.VMEM((features, features), jnp.bfloat16),
            pltpu.VMEM(w_spectrum.shape, jnp.bfloat16),
            pltpu.VMEM(w_spectrum.shape, jnp.bfloat16),
            pltpu.VMEM(w_output.shape, jnp.bfloat16),
            pltpu.VMEM(w_fourier_in.shape, jnp.bfloat16),
            pltpu.VMEM((batches, seq_local, features), jnp.bfloat16),
            pltpu.VMEM((batches, seq_local, 1), jnp.float32),
            pltpu.VMEM((channels, steps, n), jnp.float32),
            pltpu.VMEM((n, cpd, n), jnp.float32),
            pltpu.VMEM((batches, channels, steps, n), jnp.bfloat16),
            pltpu.VMEM((batches, rows, cpd, steps, n), jnp.bfloat16),
            pltpu.VMEM((batches, n, cpd, n), jnp.bfloat16),
            pltpu.VMEM((cols, batches, rows, steps, cpd, n), jnp.bfloat16),
            dma((batches, chunks)),
            dma((3,)),
            dma((batches, rows)),
            dma((batches, rows)),
            dma((batches, rows)),
            dma((cols, batches, rows)),
            dma((cols, batches, rows)),
        ],
        compiler_params=pltpu.CompilerParams(
            collective_id=0, has_side_effects=True, vmem_limit_bytes=60 * 1024 * 1024
        ),
    )(
        tokens, norm_gain[None, :], w_fourier_in, w_gate, w_spectrum, w_output,
        jnp.asarray(np.kron(np.eye(local_groups), fold), jnp.float32),
        jnp.asarray(unfold, jnp.bfloat16),
        jnp.asarray(first, jnp.bfloat16), jnp.asarray(second, jnp.bfloat16),
        jnp.asarray(twist, jnp.float32),
    )


def body(rows, cols, *args):
    tokens, w_fourier_in = args[0], args[2]
    seq_local, channels = tokens.shape[1], w_fourier_in.shape[1]
    n = int(round((seq_local * rows) ** 0.5))
    fits = (
        n * n == seq_local * rows
        and n % 128 == 0
        and channels % (16 * rows) == 0
        and channels % GROUP_WIDTH == 0
        and seq_local % (16 * n) == 0
        and cols % 2 == 0
    )
    if fits:
        return fused(rows, cols, *args)
    return on_device(*args)


def solution(mesh):
    placed = (P(None, "row", None), P(), P(None, "col"), P(), P(), P(None, "col"))
    return jax.shard_map(
        functools.partial(body, mesh.shape["row"], mesh.shape["col"]),
        mesh=mesh, in_specs=placed, out_specs=P(None, "row", "col"), check_vma=False,
    )
```

profile of v0, /device:TPU:1, one launch (start us, length us, event | category | flops | bytes accessed | tf_op | source)
XLA Modules:
  0.0 175.4 jit_solution(16493660522271949661)
XLA Ops:
  6.5 0.0 copy-start
  6.5 0.0 copy-start.2
  6.5 0.0 copy-start.5
  6.5 5.2 %fusion = f32[2,2048]{1,0:T(2,128)S(1)} fusion(bf16[2,2048,1024]{2,1,0:T(8,128)(2,1)} %param.6), kind=kLoop, calls=%fused_computation.2 | loop fusion | flops 12578816 | bytes 8404992 | tf_op jit(solution)/shard_map/reduce_sum | solution.py:63
  11.8 0.6 copy-done.2
  12.5 0.0 copy-done.5
  12.5 0.0 copy-start.4
  12.5 2.2 %fusion.2 = bf16[2,2048,1024]{2,1,0:T(8,128)(2,1)S(1)} fusion(bf16[2,2048,1024]{2,1,0:T(8,128)(2,1)S(1)} %copy-done.2, f32[1024]{0:T(1024)S(1)} %copy-done.5, f32[2,2048]{1,0:T(2,128)S(1)} %add_rsqrt_fusion), kind=kLoop, calls=%fused_computation.4 | loop fusion | flops 16777216 | bytes 16797696 | tf_op jit(solution)/shard_map/convert_element_type | solution.py:64
  14.7 0.0 copy-start.1
  14.7 3.2 %copy-done.1 = bf16[2,2048,1024]{2,1,0:T(8,128)(2,1)} copy-done((bf16[2,2048,1024]{2,1,0:T(8,128)(2,1)}, bf16[2,2048,1024]{2,1,0:T(8,128)(2,1)S(1)}, u32[]{:S(2)}) %copy-start.1) | copy-done | bytes 8388632
  17.9 0.0 copy-done.4
  17.9 2.7 %convolution_convert_fusion = bf16[4096,64]{0,1:T(8,128)(2,1)S(1)} fusion(bf16[4096,1024]{1,0:T(8,128)(2,1)S(1)} %bitcast.69, bf16[1024,64]{0,1:T(8,128)(2,1)S(1)} %copy-done.4), kind=kOutput, calls=%fused_computation.8 | convolution fusion | flops 537133056 | bytes 9043968 | tf_op jit(solution)/shard_map/dot_general | solution.py:65
  20.5 0.7 fusion.7
  21.2 1.0 convert_element_type.107
  22.2 12.0 %all-to-all-start.1 = ((bf16[32,4,2048]{2,1,0:T(4,128)(2,1)}), bf16[32,4,2048]{2,1,0:T(4,128)(2,1)S(1)}, u32[]{:S(2)}, u32[]{:S(2)}) async-start(bf16[32,4,2048]{2,1,0:T(4,128)(2,1)} %convert_element_type.107), calls=%async_computation.1 | async-start | bytes 1048576 | tf_op jit(solution)/shard_map/all_to_all | solution.py:80
  34.3 1.5 fusion.6
  35.8 2.1 %convert_element_type.103 = bf16[32,4,2048]{2,1,0:T(4,128)(2,1)} reshape(bf16[2,1,64,2048]{3,2,0,1:T(8,128)(2,1)} %fusion.6) | data formatting | bytes 1048576 | tf_op jit(solution)/shard_map/convert_element_type | solution.py:19
  37.9 12.5 %all-to-all-done.1 = bf16[32,4,2048]{2,1,0:T(4,128)(2,1)S(1)} async-done(((bf16[32,4,2048]{2,1,0:T(4,128)(2,1)}), bf16[32,4,2048]{2,1,0:T(4,128)(2,1)S(1)}, u32[]{:S(2)}, u32[]{:S(2)}) %all-to-all-start.1) | async-done | bytes 524320 | tf_op jit(solution)/shard_map/all_to_all | solution.py:80
  50.3 5.7 %all-to-all-start = ((bf16[32,4,2048]{2,1,0:T(4,128)(2,1)}), bf16[32,4,2048]{2,1,0:T(4,128)(2,1)}, u32[]{:S(2)}, u32[]{:S(2)}) async-start(bf16[32,4,2048]{2,1,0:T(4,128)(2,1)} %convert_element_type.103), calls=%async_computation | async-start | bytes 1048576 | tf_op jit(solution)/shard_map/all_to_all | solution.py:77
  56.0 0.2 all-gather.2.cloned.1.call-start
  56.3 1.0 fusion.48
  57.2 0.1 copy.17
  57.4 1.0 fusion.47
  58.3 0.8 copy.18
  59.2 0.3 copy.16
  59.5 0.2 reshape.92
  59.7 11.3 %all-to-all-done = bf16[32,4,2048]{2,1,0:T(4,128)(2,1)} async-done(((bf16[32,4,2048]{2,1,0:T(4,128)(2,1)}), bf16[32,4,2048]{2,1,0:T(4,128)(2,1)}, u32[]{:S(2)}, u32[]{:S(2)}) %all-to-all-start) | async-done | bytes 524320 | tf_op jit(solution)/shard_map/all_to_all | solution.py:77
  71.0 2.1 %copy.14 = bf16[4,32,2048]{2,1,0:T(8,128)(2,1)} copy(bf16[4,32,2048]{2,0,1:T(4,128)(2,1)} %bitcast.5) | data formatting | bytes 1048576 | tf_op jit(solution)/shard_map/all_to_all | solution.py:77
  73.2 1.3 reshape.91
  74.5 0.0 copy-start.3
  74.5 1.5 fusion.38
  76.0 1.5 fusion.36
  77.5 1.6 convolution_add_fusion
  79.1 1.6 convolution_subtract_fusion
  80.7 0.0 copy-done.3
  80.7 2.1 %fusion.12 = f32[256,4,256]{2,0,1:T(8,128)S(1)} fusion(f32[256,4,256]{2,0,1:T(8,128)S(1)} %convolution_subtract_fusion, f32[256,4,256]{2,0,1:T(8,128)S(1)} %convolution_add_fusion, f32[256,256]{1,0:T(8,128)S(1)} %copy-done.3, f32[256,256]{1,0:T(8,128)S(1)} %copy.17), kind=kOutput, calls=%fused_computation.21 | convolution fusion | flops 807010304 | bytes 3670016 | tf_op jit(solution)/shard_map/ckq,qj->cjk/dot_general | solution.py:39
  82.8 2.4 %fusion.10 = bf16[4,256,256]{2,1,0:T(8,128)(2,1)S(1)} fusion(f32[256,4,256]{2,0,1:T(8,128)S(1)} %fusion.12, f32[256,4,256]{2,0,1:T(8,128)S(1)} %convolution_add_fusion, f32[256,4,256]{2,0,1:T(8,128)S(1)} %convolution_subtract_fusion, f32[256,256]{1,0:T(8,128)S(1)} %copy-done.3, f32[256,256]{1,0:T(8,128)S(1)} %copy.17), kind=kOutput, calls=%fused_computation.19 | convolution fusion | flops 807796736 | bytes 4194304 | tf_op jit(solution)/shard_map/ckq,qj->cjk/dot_general | solution.py:39
  85.2 0.2 convert_element_type.111
  85.5 0.4 copy.19
  85.9 21.5 %all_to_all.39 = bf16[4,32,2048]{2,0,1:T(4,128)(2,1)S(1)} all-to-all(bf16[4,32,2048]{2,0,1:T(4,128)(2,1)S(1)} %copy.19), channel_id=1, replica_groups=mesh['row'=32,'col'=8] {'row'}, dimensions={1} | all-to-all | bytes 1048576 | tf_op jit(solution)/shard_map/all_to_all | solution.py:84
  107.4 0.1 reshape.93
  107.6 0.8 copy.22
  108.4 0.0 all-gather.2.cloned.1.call-update
  108.4 0.0 copy-start.6
  108.4 33.1 %all-gather.2.cloned.1.call-done = bf16[4096,512]{0,1:T(8,128)(2,1)} async-done(((bf16[4096,64]{0,1:T(8,128)(2,1)}), bf16[4096,512]{0,1:T(8,128)(2,1)}) %all-gather.2.cloned.1.call-update) | async-done | bytes 4194320 | tf_op jit(solution)/shard_map/all_gather | solution.py:23
  141.5 10.3 %fusion.102 = bf16[4096,1024]{1,0:T(8,128)(2,1)} fusion(bf16[4096,512]{0,1:T(8,128)(2,1)} %all-gather.2.cloned.1.call-done, bf16[512,1024]{1,0:T(8,128)(2,1)} %param.10), kind=kOutput, calls=%fused_computation.113 | convolution fusion | flops 4294967296 | bytes 13631488 | tf_op jit(solution)/shard_map/dot_general | solution.py:90
  151.8 0.0 copy-done
  151.8 0.0 copy-done.6
  151.8 16.7 %fusion.4 = bf16[4096,128]{1,0:T(8,128)(2,1)} fusion(bf16[1024,128]{1,0:T(8,128)(2,1)S(1)} %copy-done.6, bf16[4096,1024]{1,0:T(8,128)(2,1)} %bitcast.70, bf16[1024,1024]{1,0:T(8,128)(2,1)S(1)} %copy-done, bf16[4096,1024]{1,0:T(8,128)(2,1)} %fusion.102), kind=kOutput, calls=%fused_computation.7 | convolution fusion | flops 9689366528 | bytes 20185088 | tf_op jit(solution)/shard_map/dot_general | solution.py:97
  (1 shorter events, 0.0 us)
Async XLA Ops:
  6.5 145.3 %copy-start = (bf16[1024,1024]{1,0:T(8,128)(2,1)S(1)}, bf16[1024,1024]{1,0:T(8,128)(2,1)}, u32[]{:S(2)}) copy-start(bf16[1024,1024]{1,0:T(8,128)(2,1)} %param.9) | copy-start | bytes 6291460
  6.5 5.9 %copy-start.2 = (bf16[2,2048,1024]{2,1,0:T(8,128)(2,1)S(1)}, bf16[2,2048,1024]{2,1,0:T(8,128)(2,1)}, u32[]{:S(2)}) copy-start(bf16[2,2048,1024]{2,1,0:T(8,128)(2,1)} %param.6) | copy-start | bytes 25165828
  6.5 5.9 %copy-start.5 = (f32[1024]{0:T(1024)S(1)}, f32[1024]{0:T(1024)}, u32[]{:S(2)}) copy-start(f32[1024]{0:T(1024)} %param.7) | copy-start | bytes 12292
  12.5 5.4 %copy-start.4 = (bf16[1024,64]{0,1:T(8,128)(2,1)S(1)}, bf16[1024,64]{0,1:T(8,128)(2,1)}, u32[]{:S(2)}) copy-start(bf16[1024,64]{0,1:T(8,128)(2,1)} %param.8) | copy-start | bytes 393220
  14.7 3.2 %copy-start.1 = (bf16[2,2048,1024]{2,1,0:T(8,128)(2,1)}, bf16[2,2048,1024]{2,1,0:T(8,128)(2,1)S(1)}, u32[]{:S(2)}) copy-start(bf16[2,2048,1024]{2,1,0:T(8,128)(2,1)S(1)} %fusion.2) | copy-start | bytes 25165828
  22.2 28.1 %all-to-all-start.1 = ((bf16[32,4,2048]{2,1,0:T(4,128)(2,1)}), bf16[32,4,2048]{2,1,0:T(4,128)(2,1)S(1)}, u32[]{:S(2)}, u32[]{:S(2)}) async-start(bf16[32,4,2048]{2,1,0:T(4,128)(2,1)} %convert_element_type.107), calls=%async_computation.1 | async-start | bytes 1048576 | tf_op jit(solution)/shard_map/all_to_all | solution.py:80
  50.3 20.7 %all-to-all-start = ((bf16[32,4,2048]{2,1,0:T(4,128)(2,1)}), bf16[32,4,2048]{2,1,0:T(4,128)(2,1)}, u32[]{:S(2)}, u32[]{:S(2)}) async-start(bf16[32,4,2048]{2,1,0:T(4,128)(2,1)} %convert_element_type.103), calls=%async_computation | async-start | bytes 1048576 | tf_op jit(solution)/shard_map/all_to_all | solution.py:77
  56.0 85.5 %all-gather.2.cloned.1.call-start = ((), (), s32[]{:S(2)}) async-start(), calls=%async_computation.3 | async-start | bytes 4718592 | tf_op jit(solution)/shard_map/all_gather | solution.py:23
  74.5 6.2 %copy-start.3 = (f32[256,256]{1,0:T(8,128)S(1)}, f32[256,256]{1,0:T(8,128)}, u32[]{:S(2)}) copy-start(f32[256,256]{1,0:T(8,128)} %copy.18) | copy-start | bytes 786436
  108.4 43.4 %copy-start.6 = (bf16[1024,128]{1,0:T(8,128)(2,1)S(1)}, bf16[1024,128]{1,0:T(8,128)(2,1)}, u32[]{:S(2)}) copy-start(bf16[1024,128]{1,0:T(8,128)(2,1)} %param.11) | copy-start | bytes 786436
Sparse Core Ops, SparseCore 0:
  108.5 32.9 all-gather.1
where the time goes:
time: 176 us; the launch traced here: 175 us
  waiting for transfers between devices  56.9 us (32%)
  matrix products  42.6 us (24%)
  blocking collectives  21.5 us (12%)
  starting transfers between devices  17.9 us (10%)
  between operations  13.6 us (8%)
  local copies, waits for them, and re-layouts  13.4 us (8%)
  other arithmetic  9.39 us (5%)
    all_gather x1, waiting for transfers between devices, over_all(): lax.all_gather(part, axis, axis=dim, tiled=True)  33.1 us
    all_to_all x1, blocking collectives, on_device(): lax.all_to_all(spectrum, 'row', split_axis=1, concat_axis=0, tiled=True)  21.5 us
    dot_general x1, matrix products, on_device(): result = jnp.dot(mixed, w_output, preferred_element_type=jnp.float32)  16.7 us
    all_to_all x1, waiting for transfers between devices, on_device(): lax.all_to_all(shortened(imag_part), 'row', split_axis=0, concat_axis=1,...  12.5 us
    all_to_all x1, starting transfers between devices, on_device(): lax.all_to_all(shortened(imag_part), 'row', split_axis=0, concat_axis=1,...  12 us
    all_to_all x1, waiting for transfers between devices, on_device(): lax.all_to_all(shortened(real_part), 'row', split_axis=0, concat_axis=1,...  11.3 us
    dot_general x1, matrix products, add_spectrum(): jnp.dot(portion, weight_rows, preferred_element_type=jnp.float32)  10.3 us
    dot_general x4, matrix products, transform_first(): jnp.einsum('cpq,pk->ckq', cube, table, precision=lax.Precision.HIGHEST)  6.18 us
  transfers between devices with their start and end apart: 3, of which 3 were waited for; matrix products, arithmetic and copies ran while one was open for 4% of the time, Pallas kernels for 0%

commit v1 on v0

v1 whole, which is shorter than its diff:
```python
import functools

import jax
import jax.numpy as jnp
import numpy as np
from jax import lax
from jax.experimental import pallas as pl
from jax.experimental.pallas import tpu as pltpu
from jax.sharding import PartitionSpec as P

GROUP_WIDTH = 64
FIRST_LEN = 256
LANES = 128


norm_eps = 1e-06


def shortened(value):
    return jax.tree.map(lambda a: a.astype(jnp.bfloat16) if a.dtype == jnp.float32 else a, value)


def over_all(value, axis, dim, absorb, carry):
    whole = jax.tree.map(lambda part: lax.all_gather(part, axis, axis=dim, tiled=True), value)
    return absorb(carry, whole, jnp.int32(0))


def dft_tables(length_in, length_out, period):
    left_index = lax.broadcasted_iota(jnp.int32, (length_in, length_out), 0)
    right_index = lax.broadcasted_iota(jnp.int32, (length_in, length_out), 1)
    angles = (left_index * right_index % period).astype(jnp.float32) * (2.0 * jnp.pi / period)
    return (jnp.cos(angles), jnp.sin(angles))


def transform_first(cube, table):
    return jnp.einsum("cpq,pk->ckq", cube, table, precision=lax.Precision.HIGHEST)


def transform_second(cube, table):
    return jnp.einsum("ckq,qj->cjk", cube, table, precision=lax.Precision.HIGHEST)


def positional(real_part, imag_part):
    rows_count, seq_total = real_part.shape
    second_len = seq_total // FIRST_LEN
    cos_first, sin_first = dft_tables(FIRST_LEN, FIRST_LEN, FIRST_LEN)
    cos_twist, sin_twist = dft_tables(FIRST_LEN, second_len, seq_total)
    cos_second, sin_second = dft_tables(second_len, second_len, second_len)
    real_cube = real_part.reshape(rows_count, FIRST_LEN, second_len)
    imag_cube = imag_part.reshape(rows_count, FIRST_LEN, second_len)
    section_real = transform_first(real_cube, cos_first) + transform_first(imag_cube, sin_first)
    section_imag = transform_first(imag_cube, cos_first) - transform_first(real_cube, sin_first)
    twist_real = section_real * cos_twist + section_imag * sin_twist
    twist_imag = section_imag * cos_twist - section_real * sin_twist
    summed = transform_second(twist_real, cos_second) + transform_second(twist_imag, sin_second)
    norm_scale = 1.0 / jnp.sqrt(jnp.float32(seq_total * GROUP_WIDTH))
    return (summed.reshape(rows_count, seq_total) * norm_scale).astype(jnp.bfloat16)


def on_device(tokens, norm_gain, w_fourier_in, w_gate, w_spectrum, w_output):
    batches, seq_local, features = tokens.shape
    tokens_count = batches * seq_local
    widened = tokens.astype(jnp.float32)
    inverse = lax.rsqrt(jnp.mean(widened * widened, axis=-1, keepdims=True) + norm_eps)
    normed = (widened * inverse * norm_gain).astype(jnp.bfloat16).reshape(tokens_count, features)
    fourier_in = jnp.dot(normed, w_fourier_in, preferred_element_type=jnp.float32).astype(
        jnp.bfloat16
    )
    local_groups = w_fourier_in.shape[1] // GROUP_WIDTH
    grouped = fourier_in.astype(jnp.float32).reshape(batches, seq_local, local_groups, GROUP_WIDTH)
    cos_group, sin_group = dft_tables(GROUP_WIDTH, GROUP_WIDTH, GROUP_WIDTH)
    real_part = jnp.einsum(
        "btgn,nm->bgmt", grouped, cos_group, precision=lax.Precision.HIGHEST
    ).reshape(-1, seq_local)
    imag_part = -jnp.einsum(
        "btgn,nm->bgmt", grouped, sin_group, precision=lax.Precision.HIGHEST
    ).reshape(-1, seq_local)
    real_part = lax.all_to_all(
        shortened(real_part), "row", split_axis=0, concat_axis=1, tiled=True
    ).astype(real_part.dtype)
    imag_part = lax.all_to_all(
        shortened(imag_part), "row", split_axis=0, concat_axis=1, tiled=True
    ).astype(imag_part.dtype)
    spectrum = positional(real_part, imag_part)
    spectrum = lax.all_to_all(spectrum, "row", split_axis=1, concat_axis=0, tiled=True)
    spectrum = spectrum.reshape(batches, local_groups * GROUP_WIDTH, seq_local)
    spectrum = jnp.transpose(spectrum, (0, 2, 1)).reshape(tokens_count, local_groups * GROUP_WIDTH)

    def add_spectrum(running, portion, beginning):
        weight_rows = lax.dynamic_slice_in_dim(w_spectrum, beginning, portion.shape[1], 0)
        return running + jnp.dot(portion, weight_rows, preferred_element_type=jnp.float32)

    mixed_pre = over_all(
        spectrum, "col", 1, add_spectrum, jnp.zeros((tokens_count, features), jnp.float32)
    ).astype(jnp.bfloat16)
    gate_pre = jnp.dot(normed, w_gate, preferred_element_type=jnp.float32)
    mixed = (jax.nn.sigmoid(gate_pre) * mixed_pre.astype(jnp.float32)).astype(jnp.bfloat16)
    result = jnp.dot(mixed, w_output, preferred_element_type=jnp.float32)
    return result.astype(jnp.bfloat16).reshape(batches, seq_local, -1)


MESH = pl.DeviceIdType.MESH
HALF = GROUP_WIDTH // 2


def fold_table():
    n = np.arange(GROUP_WIDTH)
    table = np.zeros((2, HALF, GROUP_WIDTH))
    for m in range(HALF):
        table[0, m] = np.cos(2 * np.pi * (n * m % GROUP_WIDTH) / GROUP_WIDTH)
        table[1, m] = np.sin(2 * np.pi * (n * m % GROUP_WIDTH) / GROUP_WIDTH)
    table[1, 0] = np.cos(np.pi * n)
    return table.reshape(GROUP_WIDTH, GROUP_WIDTH)


def first_table(n1):
    a = np.arange(n1)
    ang = 2 * np.pi * (np.outer(a, a) % n1) / n1
    return np.concatenate([np.cos(ang), np.sin(ang)], 0)


def twist_table(n1, n2):
    phi = 2 * np.pi * np.outer(np.arange(n1), np.arange(n2)) / (n1 * n2)
    scale = 1.0 / np.sqrt(n1 * n2 * GROUP_WIDTH)
    return np.stack([np.cos(phi) * scale, np.sin(phi) * scale])


def second_table(rows, n2):
    q = np.arange(n2)
    psi = 2 * np.pi * (np.outer(q, q) % n2) / n2
    cos, sin = np.cos(psi), np.sin(psi)
    even = np.concatenate([cos, sin], 1)
    odd = np.concatenate([sin, -cos], 1)
    zero = np.zeros_like(even)
    plain = np.stack([np.concatenate([even, -odd], 1), np.concatenate([even, odd], 1)])
    first = np.stack([np.concatenate([even, zero], 1), np.concatenate([zero, even], 1)])
    both = np.stack([plain, first])
    per = n2 // rows
    both = both.reshape(2, 2, rows, per, 4 * n2).transpose(0, 3, 2, 1, 4)
    return both.reshape(2, 2 * n2, 4 * n2)


def channel_order(rows, cols):
    take = np.zeros((rows, cols, 2), np.int64)
    for r in range(rows):
        for c in range(cols):
            take[r, c, 0] = c * GROUP_WIDTH + r
            take[r, c, 1] = c * GROUP_WIDTH + (HALF if r == 0 else GROUP_WIDTH - r)
    return np.eye(rows * cols * 2)[take.reshape(-1)]


def row_offsets():
    far = lambda n: sorted(range(n), key=lambda d: -min(d, n - d))
    return [(dz, dy) for dz in far(8) for dy in far(4) if dz or dy]


def mixer_kernel(
    rows, cols, tok, gain_in, wf_in, wg_in, wspec_in, wout, fold_in, f1_in, f2_in, tw_in, perm_in, out,
    tokv, gain, wf, wg, wsv, ws, wo, fold, f1, f2, tw, perm, wp, gate, ysc, s1, x1, xs, zs, spec, osc,
    tsem, lsem, s1s, s1r, xss, xsr, s2s, s2r, oss, osr, wos, wor,
):
    batches, seq_local, features = tok.shape
    n1, n2 = tw.shape[1:]
    blocks = seq_local // n2
    span = seq_local // cols
    width = wout.shape[1]
    chunk = 512
    chunks = seq_local // chunk
    me = lax.axis_index("row")
    col = lax.axis_index("col")
    z, y = lax.div(me, 4), lax.rem(me, 4)
    sib = col + 1 - 2 * lax.rem(col, 2)
    peers = [lax.rem(z + dz, 8) * 4 + lax.rem(y + dy, 4) for dz, dy in row_offsets()]
    far = [lax.rem(col + 4, cols), lax.rem(sib + 4, cols)]
    near = [lax.rem(col + 2, cols), lax.rem(col + 6, cols), lax.rem(sib + 2, cols), lax.rem(sib + 6, cols)]
    others = far + near + [sib]

    def load(src, dst, at):
        copy = pltpu.make_async_copy(src, dst, lsem.at[at])
        copy.start()
        return copy

    def lane_block(c, size):
        return pl.ds(pl.multiple_of(c * size, size), size)

    fold_load = load(fold_in, fold, 0)
    wf_load = load(wf_in, wf, 1)
    gain_load = load(gain_in, gain, 2)
    loads = {}
    for b in range(batches):
        for j in range(chunks):
            part = pl.ds(j * chunk, chunk)
            loads[b, j] = pltpu.make_async_copy(tok.at[b, part], tokv.at[b, part], tsem.at[b, j])
            loads[b, j].start()
    wo_load = load(wout, wo.at[:, lane_block(col, width)], 3)
    wg_load = load(wg_in, wg, 4)
    spec_load = load(wspec_in, wsv, 5)
    perm_load = load(perm_in, perm, 6)
    f1_load = load(f1_in, f1, 7)
    tw_load = load(tw_in, tw, 8)
    f2_load = load(f2_in, f2, 9)

    barrier = pltpu.get_barrier_semaphore()
    for to in peers:
        pl.semaphore_signal(barrier, inc=1, device_id={"row": to}, device_id_type=MESH)
    for to in others:
        pl.semaphore_signal(barrier, inc=1, device_id={"col": to}, device_id_type=MESH)

    fold_load.wait()
    wf_load.wait()
    gain_load.wait()
    folded = jnp.zeros((GROUP_WIDTH, features), jnp.float32)
    for half in range(2):
        folded += lax.dot_general(
            fold[half], wf[...], (((1,), (1,)), ((), ())), preferred_element_type=jnp.float32
        )
    wp[...] = (folded * gain[...]).astype(jnp.bfloat16)

    def project(b):
        for j in range(chunks):
            loads[b, j].wait()
            t = tokv[b, j * chunk:(j + 1) * chunk, :]
            part = lax.dot_general(
                wp[...], t, (((1,), (1,)), ((), ())), preferred_element_type=jnp.float32
            )
            squares = jnp.zeros((chunk, LANES), jnp.float32)
            for k in range(features // LANES):
                w = t[:, k * LANES:(k + 1) * LANES].astype(jnp.float32)
                squares += w * w
            total = jnp.sum(squares.T, axis=0, keepdims=True)
            part = part * lax.rsqrt(total * (1.0 / features) + norm_eps)
            for k in range(chunk // n2):
                ysc[pl.ds(j * (chunk // n2) + k, GROUP_WIDTH, stride=blocks), :] = part[:, k * n2:(k + 1) * n2]
        for c in range(2):
            half = ysc[c * rows * blocks:(c + 1) * rows * blocks, :].reshape(rows, blocks, n2)
            s1[b, :, :, c * n2:(c + 1) * n2] = half.astype(jnp.bfloat16)

    def remote(src, dst, send, recv, to):
        return pltpu.make_async_remote_copy(
            src_ref=src, dst_ref=dst, send_sem=send, recv_sem=recv, device_id=to, device_id_type=MESH
        )

    def drain(ref, sem):
        pltpu.make_async_copy(ref, ref, sem).wait()

    def send_first(b):
        for to in peers:
            remote(s1.at[b, to], x1.at[b, me], s1s.at[b], s1r.at[b], {"row": to}).start()
        x1[b, me] = s1[b, me]

    def gates(b):
        t = tokv[b, pl.ds(pl.multiple_of(col * span, span), span), :].astype(jnp.float32)
        scale = lax.rsqrt(jnp.mean(t * t, axis=-1, keepdims=True) + norm_eps)
        normed = (t * scale * gain[...]).astype(jnp.bfloat16)
        g = jnp.dot(normed, wg[...], preferred_element_type=jnp.float32)
        gate[b] = 0.5 * jnp.tanh(0.5 * g) + 0.5

    def transform(b):
        x = x1[b].reshape(n1, 2 * n2)
        g = jnp.dot(f1[...], x, preferred_element_type=jnp.float32)
        cos, sin = tw[0], tw[1]
        parts = []
        for c in range(2):
            gc = g[:n1, c * n2:(c + 1) * n2]
            gs = g[n1:, c * n2:(c + 1) * n2]
            parts.append((gc * cos - gs * sin).astype(jnp.bfloat16))
            parts.append((-(gc * sin + gs * cos)).astype(jnp.bfloat16))
        t = jnp.concatenate(parts, axis=1)
        own = jnp.where(me == 0, 1, 0)
        o = lax.dot_general(
            f2[own], t, (((1,), (1,)), ((), ())), preferred_element_type=jnp.float32
        ).astype(jnp.bfloat16)
        for c in range(cols):
            k, h = divmod(c * span, n1)
            xs[b, c] = o[k * 2 * rows:(k + 1) * 2 * rows, h:h + span].reshape(rows, 2, span)

    def send_cross(b):
        for to in others:
            remote(xs.at[b, to], zs.at[b, :, col], xss.at[b], xsr.at[b], {"col": to}).start()
        zs[b, :, col] = xs[b, col]

    def send_second(b):
        drain(xs.at[b, pl.ds(0, cols - 1)], xsr.at[b])
        for to in peers:
            remote(zs.at[b, to], spec.at[b, me], s2s.at[b], s2r.at[b], {"row": to}).start()
        spec[b, me] = zs[b, me]

    def share(owner, at, to):
        part = wo.at[:, lane_block(owner, width)]
        return remote(part, part, wos.at[at], wor.at[at], {"col": to})

    def mix(b):
        drain(s1.at[b, pl.ds(0, rows - 1)], s2r.at[b])
        lhs = spec[b].reshape(2 * rows * cols, span)
        pre = lax.dot_general(
            lhs, ws[...], (((0,), (0,)), ((), ())), preferred_element_type=jnp.float32
        )
        return (gate[b] * pre).astype(jnp.bfloat16)

    def emit(b, mixed):
        for step in range(cols // 2):
            chip = lax.rem(lax.div(col, 2) + (2, 1, 3, 0)[step], cols // 2)
            res = jnp.dot(
                mixed, wo[:, lane_block(chip, 2 * width)], preferred_element_type=jnp.float32
            ).astype(jnp.bfloat16)
            for core in range(2):
                osc[b, chip * 2 + core] = res[:, core * width:(core + 1) * width]
            rest = pl.ds(pl.multiple_of(col * span, span), span)
            targets = (far, near[0::2], near[1::2], [sib])[step]
            for to in targets:
                remote(
                    osc.at[b, to], out.at[b, rest, :], oss.at[b], osr.at[b], {"col": to}
                ).start()
            if step == cols // 2 - 1:
                out[b, rest, :] = osc[b, col]

    project(0)
    pl.semaphore_wait(barrier, rows - 1 + cols - 1)
    send_first(0)
    wo_load.wait()
    share(col, 0, near[0]).start()
    share(col, 1, near[1]).start()
    share(col, 3, sib).start()
    for b in range(1, batches):
        project(b)
        send_first(b)
    wg_load.wait()
    for b in range(batches):
        gates(b)
    spec_load.wait()
    perm_load.wait()
    ws[...] = jnp.dot(perm[...], wsv[...], preferred_element_type=jnp.float32).astype(jnp.bfloat16)
    f1_load.wait()
    tw_load.wait()
    f2_load.wait()
    for b in range(batches):
        drain(s1.at[b, pl.ds(0, rows - 1)], s1r.at[b])
        transform(b)
        send_cross(b)
        if b == 0:
            share(col, 2, far[0]).start()
            share(near[1], 0, sib).wait_recv()
            share(near[1], 4, sib).start()
            share(near[0], 1, sib).wait_recv()
            share(near[0], 5, sib).start()
    for b in range(batches):
        send_second(b)
    share(far[0], 2, sib).wait_recv()
    share(far[0], 6, sib).start()
    for at in range(3, 7):
        share(col, at, sib).wait_recv()
    for b in range(batches):
        emit(b, mix(b))
    for b in range(batches):
        drain(osc.at[b, pl.ds(0, cols - 1)], osr.at[b])
    for b in range(batches):
        drain(s1.at[b, pl.ds(0, rows - 1)], s1s.at[b])
        drain(xs.at[b, pl.ds(0, cols - 1)], xss.at[b])
        drain(s1.at[b, pl.ds(0, rows - 1)], s2s.at[b])
        drain(osc.at[b, pl.ds(0, cols - 1)], oss.at[b])
    for at in range(7):
        share(col, at, sib).wait_send()


def fused(rows, cols, tokens, norm_gain, w_fourier_in, w_gate, w_spectrum, w_output):
    batches, seq_local, features = tokens.shape
    n2 = LANES
    n1 = seq_local * rows // n2
    blocks = seq_local // n2
    span = seq_local // cols
    width = w_output.shape[1]
    fold = fold_table()
    fold_high = fold.astype(jnp.bfloat16)
    fold_low = (fold - fold_high.astype(np.float64)).astype(jnp.bfloat16)
    tables = (
        jnp.asarray(np.stack([fold_high, fold_low])),
        jnp.asarray(first_table(n1), jnp.bfloat16),
        jnp.asarray(second_table(rows, n2), jnp.bfloat16),
        jnp.asarray(twist_table(n1, n2), jnp.float32),
        jnp.asarray(channel_order(rows, cols), jnp.bfloat16),
    )
    hbm = pl.BlockSpec(memory_space=pl.ANY)
    dma = pltpu.SemaphoreType.DMA
    half = jnp.bfloat16
    scratch = [
        (tokens.shape, half), ((1, features), jnp.float32), (w_fourier_in.shape, half),
        (w_gate.shape, half), (w_spectrum.shape, half), (w_spectrum.shape, half),
        ((features, features), half), *((t.shape, t.dtype) for t in tables),
        ((GROUP_WIDTH, features), half), ((batches, span, features), jnp.float32),
        ((GROUP_WIDTH * blocks, n2), jnp.float32),
        ((batches, rows, blocks, 2 * n2), half), ((batches, rows, blocks, 2 * n2), half),
        ((batches, cols, rows, 2, span), half), ((batches, rows, cols, 2, span), half),
        ((batches, rows, cols, 2, span), half), ((batches, cols, span, width), half),
    ]
    return pl.pallas_call(
        functools.partial(mixer_kernel, rows, cols),
        out_shape=jax.ShapeDtypeStruct((batches, seq_local, width), jnp.bfloat16),
        in_specs=[hbm] * 11,
        out_specs=pl.BlockSpec(memory_space=pltpu.VMEM),
        scratch_shapes=[pltpu.VMEM(shape, dtype) for shape, dtype in scratch] + [
            dma((batches, seq_local // 512)), dma((10,)),
            *(dma((batches,)) for _ in range(8)), dma((7,)), dma((7,)),
        ],
        compiler_params=pltpu.CompilerParams(
            collective_id=0, has_side_effects=True, vmem_limit_bytes=60 * 1024 * 1024
        ),
    )(tokens, norm_gain[None, :], w_fourier_in, w_gate, w_spectrum, w_output, *tables)


def body(rows, cols, *args):
    tokens, w_fourier_in, w_output = args[0], args[2], args[5]
    fits = (
        rows == HALF and cols == 8 and w_fourier_in.shape[1] == GROUP_WIDTH
        and tokens.shape[1:] == (16 * LANES, 8 * LANES) and w_output.shape[1] == LANES
    )
    if fits:
        return fused(rows, cols, *args)
    return on_device(*args)


def solution(mesh):
    placed = (P(None, "row", None), P(), P(None, "col"), P(), P(), P(None, "col"))
    return jax.shard_map(
        functools.partial(body, mesh.shape["row"], mesh.shape["col"]),
        mesh=mesh, in_specs=placed, out_specs=P(None, "row", "col"), check_vma=False,
    )
```

time: 176 us -> 57.2 us (0.33)
  waiting for transfers between devices: 56.9 us -> 0 us
  Pallas kernels: 0 us -> 53 us
  matrix products: 42.6 us -> 0 us
  blocking collectives: 21.5 us -> 0 us
  starting transfers between devices: 17.9 us -> 0 us
  between operations: 13.6 us -> 0.01 us
  other arithmetic: 9.39 us -> 0 us
  local copies, waits for them, and re-layouts: 13.4 us -> 4.01 us
    pallas_call x0 -> x1, Pallas kernels: none -> 53 us  [fused(): pl.pallas_call(functools.partial(mixer_kernel, rows, cols), out_shape=jax...]
    dot_general x11 -> x0, matrix products: 42.6 us -> none  [the longest x1 16.7 us: on_device(): result = jnp.dot(mixed, w_output, preferred_element_type=jnp.float32)]
    all_gather x1 -> x0, waiting for transfers between devices: 33.1 us -> none  [over_all(): lax.all_gather(part, axis, axis=dim, tiled=True)]
    all_to_all x2 -> x0, waiting for transfers between devices: 23.8 us -> none  [the longest x1 12.5 us: on_device(): lax.all_to_all(shortened(imag_part), 'row', split_axis=0, concat_axis=1,...]
    all_to_all x1 -> x0, blocking collectives: 21.5 us -> none  [on_device(): lax.all_to_all(spectrum, 'row', split_axis=1, concat_axis=0, tiled=True)]
    all_to_all x2 -> x0, starting transfers between devices: 17.7 us -> none  [the longest x1 12 us: on_device(): lax.all_to_all(shortened(imag_part), 'row', split_axis=0, concat_axis=1,...]
    reduce_sum x1 -> x0, other arithmetic: 5.25 us -> none  [on_device(): jnp.mean(widened * widened, axis=-1, keepdims=True) + norm_eps]
    convert_element_type x4 -> x0, local copies, waits for them, and re-layouts: 3.69 us -> none  [the longest x2 3.04 us: shortened(): a.astype(jnp.bfloat16)]
  transfers between devices with their start and end apart: 3 -> 0, of which waited for: 3 -> 0; matrix products, arithmetic and copies ran while one was open for 4% -> 0% of each run, Pallas kernels for 0% -> 0%
where the time goes in v1:
time: 57.2 us; the launch traced here: 57 us
  Pallas kernels  53 us (93%)
  local copies, waits for them, and re-layouts  4.01 us (7%)
    pallas_call x1, Pallas kernels, fused(): pl.pallas_call(functools.partial(mixer_kernel, rows, cols), out_shape=jax...  53 us
    unnamed x2, local copies, waits for them, and re-layouts  4.01 us

profile of v1, /device:TPU:1, one launch (start us, length us, event | category | flops | bytes accessed | tf_op | source)
XLA Modules:
  0.0 57.0 jit_solution(9317447793192918769)
XLA Ops:
  0.0 1.7 %copy.12.wf_in = bf16[1024,64]{1,0:T(8,128)(2,1)} copy(bf16[1024,64]{0,1:T(8,128)(2,1)} %param.13) | data formatting | bytes 262144 | tf_op args[2]
  1.7 53.0 %shard_map.109 = bf16[2,2048,128]{2,1,0:T(8,128)(2,1)} custom-call(bf16[2,2048,1024]{2,1,0:T(8,128)(2,1)} %tok.1, f32[1,1024]{1,0:T(1,128)} %bitcast.1, bf16[1024,64]{1,0:T(8,128)(2,1)} %copy.12.wf_in, bf16[1024,1024]{1,0:T(8,128)(2,1)} %wg_in.1, bf16[512,1024]{1,0:T(8,128)(2,1)} %wspec_in.1, bf16[1024,128]{1,0:T(8,128)(2,1)} %wout.1, ...), custom_call_target="tpu_custom_call" | custom-call | tf_op jit(solution)/shard_map/pallas_call | solution.py:395
  54.8 2.3 %copy.14 = bf16[2,2048,128]{2,1,0:T(8,128)(2,1)} copy(bf16[2,2048,128]{2,1,0:T(8,128)(2,1)} %shard_map.109) | data formatting | bytes 2097152

commit v2 on v1

--- a/solution.py
+++ b/solution.py
@@ -156,8 +156,8 @@
 
 def mixer_kernel(
     rows, cols, tok, gain_in, wf_in, wg_in, wspec_in, wout, fold_in, f1_in, f2_in, tw_in, perm_in, out,
-    tokv, gain, wf, wg, wsv, ws, wo, fold, f1, f2, tw, perm, wp, gate, ysc, s1, x1, xs, zs, spec, osc,
-    tsem, lsem, s1s, s1r, xss, xsr, s2s, s2r, oss, osr, wos, wor,
+    tokv, gain, wf, wg, wsv, ws, wo, fold, f1, f2, tw, perm, wp, gate, ysc, s1, x1, xs, ps, spec, osc,
+    tsem, lsem, s1s, s1r, sws, swr, s2s, s2r, oss, osr, wos, wor,
 ):
     batches, seq_local, features = tok.shape
     n1, n2 = tw.shape[1:]
@@ -174,6 +174,8 @@
     far = [lax.rem(col + 4, cols), lax.rem(sib + 4, cols)]
     near = [lax.rem(col + 2, cols), lax.rem(col + 6, cols), lax.rem(sib + 2, cols), lax.rem(sib + 6, cols)]
     others = far + near + [sib]
+    same = [far[0], near[0], near[1]]
+    core = lax.rem(col, 2)
 
     def load(src, dst, at):
         copy = pltpu.make_async_copy(src, dst, lsem.at[at])
@@ -212,7 +214,7 @@
     folded = jnp.zeros((GROUP_WIDTH, features), jnp.float32)
     for half in range(2):
         folded += lax.dot_general(
-            fold[half], wf[...], (((1,), (1,)), ((), ())), preferred_element_type=jnp.float32
+            fold[half], wf[...], (((1,), (0,)), ((), ())), preferred_element_type=jnp.float32
         )
     wp[...] = (folded * gain[...]).astype(jnp.bfloat16)
 
@@ -269,28 +271,45 @@
         own = jnp.where(me == 0, 1, 0)
         o = lax.dot_general(
             f2[own], t, (((1,), (1,)), ((), ())), preferred_element_type=jnp.float32
-        ).astype(jnp.bfloat16)
-        for c in range(cols):
-            k, h = divmod(c * span, n1)
-            xs[b, c] = o[k * 2 * rows:(k + 1) * 2 * rows, h:h + span].reshape(rows, 2, span)
-
-    def send_cross(b):
-        for to in others:
-            remote(xs.at[b, to], zs.at[b, :, col], xss.at[b], xsr.at[b], {"col": to}).start()
-        zs[b, :, col] = xs[b, col]
+        )
+        low, high = o[:, :span], o[:, span:]
+        mine = jnp.where(core == 0, low, high)
+        other = jnp.where(core == 0, high, low)
+        ps[b, :, core] = mine.astype(jnp.bfloat16).reshape(rows * cols // 2, 2, span)
+        xs[b] = other.astype(jnp.bfloat16).reshape(rows * cols // 2, 2, span)
+
+    def swap(b):
+        return remote(
+            xs.at[b], ps.at[b, :, core], sws.at[b], swr.at[b], {"col": sib}
+        )
 
     def send_second(b):
-        drain(xs.at[b, pl.ds(0, cols - 1)], xsr.at[b])
-        for to in peers:
-            remote(zs.at[b, to], spec.at[b, me], s2s.at[b], s2r.at[b], {"row": to}).start()
-        spec[b, me] = zs[b, me]
+        def one(to, c):
+            remote(
+                ps.at[b, lax.div(c, 2) * rows + to], spec.at[b, me, lax.div(col, 2)],
+                s2s.at[b], s2r.at[b], {"row": to, "col": c},
+            ).start()
+
+        def per_row(i, carry):
+            step = lax.div(i, 4)
+            dz = 4 + lax.div(step + 1, 2) * (1 - 2 * lax.rem(step, 2))
+            dy = 2 + lax.div(lax.rem(i, 4) + 1, 2) * (1 - 2 * lax.rem(i, 2))
+            to = lax.rem(z + dz, 8) * 4 + lax.rem(y + dy, 4)
+            for c in same:
+                one(to, c)
+            one(to, col)
+            return carry
+
+        lax.fori_loop(0, rows - 1, per_row, 0)
+        for c in same:
+            one(me, c)
+        spec[b, me, lax.div(col, 2)] = ps[b, lax.div(col, 2) * rows + me]
 
     def share(owner, at, to):
         part = wo.at[:, lane_block(owner, width)]
         return remote(part, part, wos.at[at], wor.at[at], {"col": to})
 
     def mix(b):
-        drain(s1.at[b, pl.ds(0, rows - 1)], s2r.at[b])
         lhs = spec[b].reshape(2 * rows * cols, span)
         pre = lax.dot_general(
             lhs, ws[...], (((0,), (0,)), ((), ())), preferred_element_type=jnp.float32
@@ -314,52 +333,76 @@
             if step == cols // 2 - 1:
                 out[b, rest, :] = osc[b, col]
 
-    project(0)
-    pl.semaphore_wait(barrier, rows - 1 + cols - 1)
-    send_first(0)
+    scope = jax.named_scope
+    with scope("project0"):
+        project(0)
+    with scope("barrier"):
+        pl.semaphore_wait(barrier, rows - 1 + cols - 1)
+    with scope("send0"):
+        send_first(0)
     wo_load.wait()
     share(col, 0, near[0]).start()
     share(col, 1, near[1]).start()
+    share(col, 2, far[0]).start()
     share(col, 3, sib).start()
+    with scope("gates"):
+        wg_load.wait()
+        gates(0)
+    with scope("spectrum_rows"):
+        spec_load.wait()
+        perm_load.wait()
+        ws[...] = jnp.dot(
+            perm[...], wsv[...], preferred_element_type=jnp.float32
+        ).astype(jnp.bfloat16)
+        f1_load.wait()
+        tw_load.wait()
+        f2_load.wait()
     for b in range(1, batches):
-        project(b)
-        send_first(b)
-    wg_load.wait()
+        with scope("project%d" % b):
+            project(b)
+        with scope("send%d" % b):
+            send_first(b)
+        with scope("gates"):
+            gates(b)
     for b in range(batches):
-        gates(b)
-    spec_load.wait()
-    perm_load.wait()
-    ws[...] = jnp.dot(perm[...], wsv[...], preferred_element_type=jnp.float32).astype(jnp.bfloat16)
-    f1_load.wait()
-    tw_load.wait()
-    f2_load.wait()
+        with scope("wait_first%d" % b):
+            drain(s1.at[b, pl.ds(0, rows - 1)], s1r.at[b])
+        with scope("transform%d" % b):
+            transform(b)
+        with scope("swap%d" % b):
+            swap(b).start()
+            swap(b).wait_recv()
+        with scope("second%d" % b):
+            send_second(b)
+        if b == 0:
+            with scope("share"):
+                share(near[1], 0, sib).wait_recv()
+                share(near[1], 4, sib).start()
+                share(near[0], 1, sib).wait_recv()
+                share(near[0], 5, sib).start()
+    with scope("share2"):
+        share(far[0], 2, sib).wait_recv()
+        share(far[0], 6, sib).start()
+        for at in range(3, 7):
+            share(col, at, sib).wait_recv()
     for b in range(batches):
-        drain(s1.at[b, pl.ds(0, rows - 1)], s1r.at[b])
-        transform(b)
-        send_cross(b)
-        if b == 0:
-            share(col, 2, far[0]).start()
-            share(near[1], 0, sib).wait_recv()
-            share(near[1], 4, sib).start()
-            share(near[0], 1, sib).wait_recv()
-            share(near[0], 5, sib).start()
-    for b in range(batches):
-        send_second(b)
-    share(far[0], 2, sib).wait_recv()
-    share(far[0], 6, sib).start()
-    for at in range(3, 7):
-        share(col, at, sib).wait_recv()
-    for b in range(batches):
-        emit(b, mix(b))
-    for b in range(batches):
-        drain(osc.at[b, pl.ds(0, cols - 1)], osr.at[b])
-    for b in range(batches):
-        drain(s1.at[b, pl.ds(0, rows - 1)], s1s.at[b])
-        drain(xs.at[b, pl.ds(0, cols - 1)], xss.at[b])
-        drain(s1.at[b, pl.ds(0, rows - 1)], s2s.at[b])
-        drain(osc.at[b, pl.ds(0, cols - 1)], oss.at[b])
-    for at in range(7):
-        share(col, at, sib).wait_send()
+        with scope("wait_second%d" % b):
+            drain(ps.at[b, pl.ds(0, rows * cols // 2 - 1)], s2r.at[b])
+        with scope("mix%d" % b):
+            mixed = mix(b)
+        with scope("emit%d" % b):
+            emit(b, mixed)
+    with scope("wait_out"):
+        for b in range(batches):
+            drain(osc.at[b, pl.ds(0, cols - 1)], osr.at[b])
+    with scope("tail"):
+        for b in range(batches):
+            drain(s1.at[b, pl.ds(0, rows - 1)], s1s.at[b])
+            drain(ps.at[b, pl.ds(0, rows * cols // 2 - 1)], s2s.at[b])
+            swap(b).wait_send()
+            drain(osc.at[b, pl.ds(0, cols - 1)], oss.at[b])
+        for at in range(7):
+            share(col, at, sib).wait_send()
 
 
 def fused(rows, cols, tokens, norm_gain, w_fourier_in, w_gate, w_spectrum, w_output):
@@ -379,22 +422,24 @@
         jnp.asarray(twist_table(n1, n2), jnp.float32),
         jnp.asarray(channel_order(rows, cols), jnp.bfloat16),
     )
-    hbm = pl.BlockSpec(memory_space=pl.ANY)
+    hbm = pl.BlockSpec(memory_space=pltpu.HBM)
     dma = pltpu.SemaphoreType.DMA
     half = jnp.bfloat16
     scratch = [
-        (tokens.shape, half), ((1, features), jnp.float32), (w_fourier_in.shape, half),
+        (tokens.shape, half), ((1, features), jnp.float32), (w_fourier_in.shape[::-1], half),
         (w_gate.shape, half), (w_spectrum.shape, half), (w_spectrum.shape, half),
         ((features, features), half), *((t.shape, t.dtype) for t in tables),
         ((GROUP_WIDTH, features), half), ((batches, span, features), jnp.float32),
         ((GROUP_WIDTH * blocks, n2), jnp.float32),
         ((batches, rows, blocks, 2 * n2), half), ((batches, rows, blocks, 2 * n2), half),
-        ((batches, cols, rows, 2, span), half), ((batches, rows, cols, 2, span), half),
-        ((batches, rows, cols, 2, span), half), ((batches, cols, span, width), half),
+        ((batches, cols // 2 * rows, 2, span), half),
+        ((batches, cols // 2 * rows, 2, 2, span), half),
+        ((batches, rows, cols // 2, 2, 2, span), half),
+        ((batches, cols, span, width), half),
     ]
     return pl.pallas_call(
         functools.partial(mixer_kernel, rows, cols),
-        out_shape=jax.ShapeDtypeStruct((batches, seq_local, width), jnp.bfloat16),
+        out_shape=pltpu.VMEM((batches, seq_local, width), jnp.bfloat16),
         in_specs=[hbm] * 11,
         out_specs=pl.BlockSpec(memory_space=pltpu.VMEM),
         scratch_shapes=[pltpu.VMEM(shape, dtype) for shape, dtype in scratch] + [
@@ -402,9 +447,9 @@
             *(dma((batches,)) for _ in range(8)), dma((7,)), dma((7,)),
         ],
         compiler_params=pltpu.CompilerParams(
-            collective_id=0, has_side_effects=True, vmem_limit_bytes=60 * 1024 * 1024
+            collective_id=0, has_side_effects=True, vmem_limit_bytes=62 * 1024 * 1024
         ),
-    )(tokens, norm_gain[None, :], w_fourier_in, w_gate, w_spectrum, w_output, *tables)
+    )(tokens, norm_gain[None, :], w_fourier_in.T, w_gate, w_spectrum, w_output, *tables)
 
 
 def body(rows, cols, *args):

time: 57.2 us -> 49.9 us (0.87)
  Pallas kernels: 53 us -> 48.8 us
  local copies, waits for them, and re-layouts: 4.01 us -> 0.97 us
    pallas_call x1, Pallas kernels: 53 us -> 48.8 us  [fused(): pl.pallas_call(functools.partial(mixer_kernel, rows, cols), out_shape=plt...]
    unnamed x2 -> x1, local copies, waits for them, and re-layouts: 4.01 us -> 0.97 us
where the time goes in v2:
time: 49.9 us; the launch traced here: 49.8 us
  Pallas kernels  48.8 us (98%)
  local copies, waits for them, and re-layouts  0.97 us (2%)
    pallas_call x1, Pallas kernels, fused(): pl.pallas_call(functools.partial(mixer_kernel, rows, cols), out_shape=plt...  48.8 us

profile of v2, /device:TPU:1, one launch (start us, length us, event | category | flops | bytes accessed | tf_op | source)
XLA Modules:
  0.0 49.8 jit_solution(5017228388576688562)
XLA Ops:
  0.0 48.8 %shard_map.109 = bf16[2,2048,128]{2,1,0:T(8,128)(2,1)S(1)} custom-call(bf16[2,2048,1024]{2,1,0:T(8,128)(2,1)} %tok.1, f32[1,1024]{1,0:T(1,128)} %bitcast.3, bf16[64,1024]{1,0:T(8,128)(2,1)} %bitcast.2, bf16[1024,1024]{1,0:T(8,128)(2,1)} %wg_in.1, bf16[512,1024]{1,0:T(8,128)(2,1)} %wspec_in.1, bf16[1024,128]{1,0:T(8,128)(2,1)} %wout.1, ...), custom_call_target="tpu_custom_call" | custom-call | tf_op jit(solution)/shard_map/pallas_call | solution.py:440
  48.8 1.0 %copy.13 = bf16[2,2048,128]{2,1,0:T(8,128)(2,1)} copy(bf16[2,2048,128]{2,1,0:T(8,128)(2,1)S(1)} %shard_map.109) | data formatting | bytes 2097152

commit v3 on v2

--- a/solution.py
+++ b/solution.py
@@ -144,19 +144,20 @@
     take = np.zeros((rows, cols, 2), np.int64)
     for r in range(rows):
         for c in range(cols):
-            take[r, c, 0] = c * GROUP_WIDTH + r
-            take[r, c, 1] = c * GROUP_WIDTH + (HALF if r == 0 else GROUP_WIDTH - r)
+            group = (c + 1 - 2 * (c % 2)) * GROUP_WIDTH
+            take[r, c, 0] = group + r
+            take[r, c, 1] = group + (HALF if r == 0 else GROUP_WIDTH - r)
     return np.eye(rows * cols * 2)[take.reshape(-1)]
 
 
 def row_offsets():
     far = lambda n: sorted(range(n), key=lambda d: -min(d, n - d))
-    return [(dz, dy) for dz in far(8) for dy in far(4) if dz or dy]
+    return [(dz, dy) for dy in far(4) for dz in far(8) if dz or dy]
 
 
 def mixer_kernel(
     rows, cols, tok, gain_in, wf_in, wg_in, wspec_in, wout, fold_in, f1_in, f2_in, tw_in, perm_in, out,
-    tokv, gain, wf, wg, wsv, ws, wo, fold, f1, f2, tw, perm, wp, gate, ysc, s1, x1, xs, ps, spec, osc,
+    tokv, gain, wf, wg, wsv, ws, wo, fold, f1, f2, tw, perm, wp, gate, ysc, tt, s1, x1, xs, ps, spec, osc,
     tsem, lsem, s1s, s1r, sws, swr, s2s, s2r, oss, osr, wos, wor,
 ):
     batches, seq_local, features = tok.shape
@@ -174,8 +175,10 @@
     far = [lax.rem(col + 4, cols), lax.rem(sib + 4, cols)]
     near = [lax.rem(col + 2, cols), lax.rem(col + 6, cols), lax.rem(sib + 2, cols), lax.rem(sib + 6, cols)]
     others = far + near + [sib]
-    same = [far[0], near[0], near[1]]
+    across = [far[1], near[2], near[3]]
     core = lax.rem(col, 2)
+
+    turns = [z * 4 + lax.rem(y + d, 4) for d in range(1, 4)]
 
     def load(src, dst, at):
         copy = pltpu.make_async_copy(src, dst, lsem.at[at])
@@ -184,6 +187,16 @@
 
     def lane_block(c, size):
         return pl.ds(pl.multiple_of(c * size, size), size)
+
+    barrier = pltpu.get_barrier_semaphore()
+    for to in peers:
+        pl.semaphore_signal(
+            barrier, inc=1, device_id={"row": to, "col": sib}, device_id_type=MESH
+        )
+    for to in turns:
+        pl.semaphore_signal(barrier, inc=1, device_id={"row": to}, device_id_type=MESH)
+    for to in others:
+        pl.semaphore_signal(barrier, inc=1, device_id={"col": to}, device_id_type=MESH)
 
     fold_load = load(fold_in, fold, 0)
     wf_load = load(wf_in, wf, 1)
@@ -201,12 +214,6 @@
     f1_load = load(f1_in, f1, 7)
     tw_load = load(tw_in, tw, 8)
     f2_load = load(f2_in, f2, 9)
-
-    barrier = pltpu.get_barrier_semaphore()
-    for to in peers:
-        pl.semaphore_signal(barrier, inc=1, device_id={"row": to}, device_id_type=MESH)
-    for to in others:
-        pl.semaphore_signal(barrier, inc=1, device_id={"col": to}, device_id_type=MESH)
 
     fold_load.wait()
     wf_load.wait()
@@ -246,9 +253,8 @@
         pltpu.make_async_copy(ref, ref, sem).wait()
 
     def send_first(b):
-        for to in peers:
-            remote(s1.at[b, to], x1.at[b, me], s1s.at[b], s1r.at[b], {"row": to}).start()
-        x1[b, me] = s1[b, me]
+        for to in peers + [me]:
+            remote(s1.at[b, to], x1.at[b, me], s1s.at[b], s1r.at[b], {"row": to, "col": sib}).start()
 
     def gates(b):
         t = tokv[b, pl.ds(pl.multiple_of(col * span, span), span), :].astype(jnp.float32)
@@ -261,22 +267,23 @@
         x = x1[b].reshape(n1, 2 * n2)
         g = jnp.dot(f1[...], x, preferred_element_type=jnp.float32)
         cos, sin = tw[0], tw[1]
-        parts = []
         for c in range(2):
             gc = g[:n1, c * n2:(c + 1) * n2]
             gs = g[n1:, c * n2:(c + 1) * n2]
-            parts.append((gc * cos - gs * sin).astype(jnp.bfloat16))
-            parts.append((-(gc * sin + gs * cos)).astype(jnp.bfloat16))
-        t = jnp.concatenate(parts, axis=1)
+            tt[:, 2 * c * n2:(2 * c + 1) * n2] = (gc * cos - gs * sin).astype(jnp.bfloat16)
+            tt[:, (2 * c + 1) * n2:(2 * c + 2) * n2] = (-(gc * sin + gs * cos)).astype(jnp.bfloat16)
         own = jnp.where(me == 0, 1, 0)
-        o = lax.dot_general(
-            f2[own], t, (((1,), (1,)), ((), ())), preferred_element_type=jnp.float32
-        )
-        low, high = o[:, :span], o[:, span:]
-        mine = jnp.where(core == 0, low, high)
-        other = jnp.where(core == 0, high, low)
-        ps[b, :, core] = mine.astype(jnp.bfloat16).reshape(rows * cols // 2, 2, span)
-        xs[b] = other.astype(jnp.bfloat16).reshape(rows * cols // 2, 2, span)
+
+        def half(which):
+            o = lax.dot_general(
+                f2[own], tt[pl.ds(pl.multiple_of(which * span, span), span), :],
+                (((1,), (1,)), ((), ())), preferred_element_type=jnp.float32,
+            )
+            return o.astype(jnp.bfloat16).reshape(rows * cols // 2, 2, span)
+
+        xs[b] = half(core)
+        swap(b).start()
+        ps[b, :, core] = half(1 - core)
 
     def swap(b):
         return remote(
@@ -290,24 +297,18 @@
                 s2s.at[b], s2r.at[b], {"row": to, "col": c},
             ).start()
 
-        def per_row(i, carry):
-            step = lax.div(i, 4)
-            dz = 4 + lax.div(step + 1, 2) * (1 - 2 * lax.rem(step, 2))
-            dy = 2 + lax.div(lax.rem(i, 4) + 1, 2) * (1 - 2 * lax.rem(i, 2))
-            to = lax.rem(z + dz, 8) * 4 + lax.rem(y + dy, 4)
-            for c in same:
+        for c in across + [sib]:
+            for to in peers + [me]:
                 one(to, c)
-            one(to, col)
-            return carry
-
-        lax.fori_loop(0, rows - 1, per_row, 0)
-        for c in same:
-            one(me, c)
-        spec[b, me, lax.div(col, 2)] = ps[b, lax.div(col, 2) * rows + me]
 
     def share(owner, at, to):
         part = wo.at[:, lane_block(owner, width)]
         return remote(part, part, wos.at[at], wor.at[at], {"col": to})
+
+    def quarter(owner, at_y, at, to):
+        size = wo.shape[0] // 4
+        part = wo.at[pl.ds(pl.multiple_of(at_y * size, size), size), lane_block(owner, width)]
+        return remote(part, part, wos.at[at], wor.at[at], to)
 
     def mix(b):
         lhs = spec[b].reshape(2 * rows * cols, span)
@@ -337,13 +338,13 @@
     with scope("project0"):
         project(0)
     with scope("barrier"):
-        pl.semaphore_wait(barrier, rows - 1 + cols - 1)
+        pl.semaphore_wait(barrier, rows - 1 + len(turns) + cols - 1)
     with scope("send0"):
         send_first(0)
     wo_load.wait()
+    quarter(col, y, 7, {"col": far[0]}).start()
     share(col, 0, near[0]).start()
     share(col, 1, near[1]).start()
-    share(col, 2, far[0]).start()
     share(col, 3, sib).start()
     with scope("gates"):
         wg_load.wait()
@@ -364,13 +365,16 @@
             send_first(b)
         with scope("gates"):
             gates(b)
+    with scope("turn"):
+        quarter(far[0], y, 7, {"col": sib}).wait_recv()
+        for d in (2, 1, 3):
+            quarter(far[0], y, 7 + d, {"row": turns[d - 1]}).start()
     for b in range(batches):
         with scope("wait_first%d" % b):
-            drain(s1.at[b, pl.ds(0, rows - 1)], s1r.at[b])
+            drain(s1.at[b], s1r.at[b])
         with scope("transform%d" % b):
             transform(b)
         with scope("swap%d" % b):
-            swap(b).start()
             swap(b).wait_recv()
         with scope("second%d" % b):
             send_second(b)
@@ -381,13 +385,14 @@
                 share(near[0], 1, sib).wait_recv()
                 share(near[0], 5, sib).start()
     with scope("share2"):
-        share(far[0], 2, sib).wait_recv()
-        share(far[0], 6, sib).start()
-        for at in range(3, 7):
+        for d in range(1, 4):
+            quarter(far[0], y, 7 + d, {"row": turns[d - 1]}).wait_recv()
+        share(far[0], 2, sib).start()
+        for at in range(2, 6):
             share(col, at, sib).wait_recv()
     for b in range(batches):
         with scope("wait_second%d" % b):
-            drain(ps.at[b, pl.ds(0, rows * cols // 2 - 1)], s2r.at[b])
+            drain(ps.at[b], s2r.at[b])
         with scope("mix%d" % b):
             mixed = mix(b)
         with scope("emit%d" % b):
@@ -397,12 +402,14 @@
             drain(osc.at[b, pl.ds(0, cols - 1)], osr.at[b])
     with scope("tail"):
         for b in range(batches):
-            drain(s1.at[b, pl.ds(0, rows - 1)], s1s.at[b])
-            drain(ps.at[b, pl.ds(0, rows * cols // 2 - 1)], s2s.at[b])
+            drain(s1.at[b], s1s.at[b])
+            drain(ps.at[b], s2s.at[b])
             swap(b).wait_send()
             drain(osc.at[b, pl.ds(0, cols - 1)], oss.at[b])
-        for at in range(7):
+        for at in range(6):
             share(col, at, sib).wait_send()
+        for at in range(7, 11):
+            quarter(col, y, at, {"col": sib}).wait_send()
 
 
 def fused(rows, cols, tokens, norm_gain, w_fourier_in, w_gate, w_spectrum, w_output):
@@ -430,7 +437,7 @@
         (w_gate.shape, half), (w_spectrum.shape, half), (w_spectrum.shape, half),
         ((features, features), half), *((t.shape, t.dtype) for t in tables),
         ((GROUP_WIDTH, features), half), ((batches, span, features), jnp.float32),
-        ((GROUP_WIDTH * blocks, n2), jnp.float32),
+        ((GROUP_WIDTH * blocks, n2), jnp.float32), ((n1, 4 * n2), half),
         ((batches, rows, blocks, 2 * n2), half), ((batches, rows, blocks, 2 * n2), half),
         ((batches, cols // 2 * rows, 2, span), half),
         ((batches, cols // 2 * rows, 2, 2, span), half),
@@ -444,7 +451,7 @@
         out_specs=pl.BlockSpec(memory_space=pltpu.VMEM),
         scratch_shapes=[pltpu.VMEM(shape, dtype) for shape, dtype in scratch] + [
             dma((batches, seq_local // 512)), dma((10,)),
-            *(dma((batches,)) for _ in range(8)), dma((7,)), dma((7,)),
+            *(dma((batches,)) for _ in range(8)), dma((11,)), dma((11,)),
         ],
         compiler_params=pltpu.CompilerParams(
             collective_id=0, has_side_effects=True, vmem_limit_bytes=62 * 1024 * 1024

time: 49.9 us -> 48.9 us (0.980)
  Pallas kernels: 48.8 us -> 47.9 us
    pallas_call x1, Pallas kernels: 48.8 us -> 47.9 us  [fused(): pl.pallas_call(functools.partial(mixer_kernel, rows, cols), out_shape=plt...]
where the time goes in v3:
time: 48.9 us; the launch traced here: 48.8 us
  Pallas kernels  47.9 us (98%)
  local copies, waits for them, and re-layouts  0.97 us (2%)
    pallas_call x1, Pallas kernels, fused(): pl.pallas_call(functools.partial(mixer_kernel, rows, cols), out_shape=plt...  47.9 us

profile of v3, /device:TPU:1, one launch (start us, length us, event | category | flops | bytes accessed | tf_op | source)
XLA Modules:
  0.0 48.8 jit_solution(4770500526265748640)
XLA Ops:
  0.0 47.9 %shard_map.109 = bf16[2,2048,128]{2,1,0:T(8,128)(2,1)S(1)} custom-call(bf16[2,2048,1024]{2,1,0:T(8,128)(2,1)} %tok.1, f32[1,1024]{1,0:T(1,128)} %bitcast.3, bf16[64,1024]{1,0:T(8,128)(2,1)} %bitcast.2, bf16[1024,1024]{1,0:T(8,128)(2,1)} %wg_in.1, bf16[512,1024]{1,0:T(8,128)(2,1)} %wspec_in.1, bf16[1024,128]{1,0:T(8,128)(2,1)} %wout.1, ...), custom_call_target="tpu_custom_call" | custom-call | tf_op jit(solution)/shard_map/pallas_call | solution.py:447
  47.9 1.0 %copy.13 = bf16[2,2048,128]{2,1,0:T(8,128)(2,1)} copy(bf16[2,2048,128]{2,1,0:T(8,128)(2,1)S(1)} %shard_map.109) | data formatting | bytes 2097152

commit v4 on v3

--- a/solution.py
+++ b/solution.py
@@ -158,7 +158,7 @@
 def mixer_kernel(
     rows, cols, tok, gain_in, wf_in, wg_in, wspec_in, wout, fold_in, f1_in, f2_in, tw_in, perm_in, out,
     tokv, gain, wf, wg, wsv, ws, wo, fold, f1, f2, tw, perm, wp, gate, ysc, tt, s1, x1, xs, ps, spec, osc,
-    tsem, lsem, s1s, s1r, sws, swr, s2s, s2r, oss, osr, wos, wor,
+    tsem, lsem, s1s, s1r, sws, swr, s2s, s2r, oss, osr, wos, wor, ready,
 ):
     batches, seq_local, features = tok.shape
     n1, n2 = tw.shape[1:]
@@ -178,6 +178,8 @@
     across = [far[1], near[2], near[3]]
     core = lax.rem(col, 2)
 
+    line = [lax.rem(z + dz, 8) * 4 + y for dz, dy in row_offsets() if dy == 0]
+    aside = [lax.rem(z + dz, 8) * 4 + lax.rem(y + dy, 4) for dz, dy in row_offsets() if dy]
     turns = [z * 4 + lax.rem(y + d, 4) for d in range(1, 4)]
 
     def load(src, dst, at):
@@ -189,7 +191,7 @@
         return pl.ds(pl.multiple_of(c * size, size), size)
 
     barrier = pltpu.get_barrier_semaphore()
-    for to in peers:
+    for to in line:
         pl.semaphore_signal(
             barrier, inc=1, device_id={"row": to, "col": sib}, device_id_type=MESH
         )
@@ -252,8 +254,8 @@
     def drain(ref, sem):
         pltpu.make_async_copy(ref, ref, sem).wait()
 
-    def send_first(b):
-        for to in peers + [me]:
+    def send_first(b, targets):
+        for to in targets:
             remote(s1.at[b, to], x1.at[b, me], s1s.at[b], s1r.at[b], {"row": to, "col": sib}).start()
 
     def gates(b):
@@ -338,14 +340,25 @@
     with scope("project0"):
         project(0)
     with scope("barrier"):
-        pl.semaphore_wait(barrier, rows - 1 + len(turns) + cols - 1)
+        pl.semaphore_wait(barrier, len(line) + len(turns) + cols - 1)
+    for to in turns:
+        pl.semaphore_signal(ready, inc=1, device_id={"row": to}, device_id_type=MESH)
     with scope("send0"):
-        send_first(0)
+        send_first(0, line)
+    with scope("ready"):
+        pl.semaphore_wait(ready, len(turns))
+    with scope("send0b"):
+        send_first(0, aside + [me])
     wo_load.wait()
     quarter(col, y, 7, {"col": far[0]}).start()
     share(col, 0, near[0]).start()
     share(col, 1, near[1]).start()
     share(col, 3, sib).start()
+    for b in range(1, batches):
+        with scope("project%d" % b):
+            project(b)
+        with scope("send%d" % b):
+            send_first(b, peers + [me])
     with scope("gates"):
         wg_load.wait()
         gates(0)
@@ -358,12 +371,8 @@
         f1_load.wait()
         tw_load.wait()
         f2_load.wait()
-    for b in range(1, batches):
-        with scope("project%d" % b):
-            project(b)
-        with scope("send%d" % b):
-            send_first(b)
-        with scope("gates"):
+    with scope("gates"):
+        for b in range(1, batches):
             gates(b)
     with scope("turn"):
         quarter(far[0], y, 7, {"col": sib}).wait_recv()
@@ -451,7 +460,7 @@
         out_specs=pl.BlockSpec(memory_space=pltpu.VMEM),
         scratch_shapes=[pltpu.VMEM(shape, dtype) for shape, dtype in scratch] + [
             dma((batches, seq_local // 512)), dma((10,)),
-            *(dma((batches,)) for _ in range(8)), dma((11,)), dma((11,)),
+            *(dma((batches,)) for _ in range(8)), dma((11,)), dma((11,)), pltpu.SemaphoreType.REGULAR,
         ],
         compiler_params=pltpu.CompilerParams(
             collective_id=0, has_side_effects=True, vmem_limit_bytes=62 * 1024 * 1024

time: 48.9 us -> 48 us (0.982)
  Pallas kernels: 47.9 us -> 46.9 us
    pallas_call x1, Pallas kernels: 47.9 us -> 46.9 us  [fused(): pl.pallas_call(functools.partial(mixer_kernel, rows, cols), out_shape=plt...]
where the time goes in v4:
time: 48 us; the launch traced here: 47.9 us
  Pallas kernels  46.9 us (98%)
  local copies, waits for them, and re-layouts  0.97 us (2%)
    pallas_call x1, Pallas kernels, fused(): pl.pallas_call(functools.partial(mixer_kernel, rows, cols), out_shape=plt...  46.9 us
    unnamed x1, local copies, waits for them, and re-layouts  0.97 us

profile of v4, /device:TPU:1, one launch (start us, length us, event | category | flops | bytes accessed | tf_op | source)
XLA Modules:
  0.0 47.9 jit_solution(562411698332740778)
XLA Ops:
  0.0 46.9 %shard_map.109 = bf16[2,2048,128]{2,1,0:T(8,128)(2,1)S(1)} custom-call(bf16[2,2048,1024]{2,1,0:T(8,128)(2,1)} %tok.1, f32[1,1024]{1,0:T(1,128)} %bitcast.3, bf16[64,1024]{1,0:T(8,128)(2,1)} %bitcast.2, bf16[1024,1024]{1,0:T(8,128)(2,1)} %wg_in.1, bf16[512,1024]{1,0:T(8,128)(2,1)} %wspec_in.1, bf16[1024,128]{1,0:T(8,128)(2,1)} %wout.1, ...), custom_call_target="tpu_custom_call" | custom-call | tf_op jit(solution)/shard_map/pallas_call | solution.py:456
  46.9 1.0 %copy.13 = bf16[2,2048,128]{2,1,0:T(8,128)(2,1)} copy(bf16[2,2048,128]{2,1,0:T(8,128)(2,1)S(1)} %shard_map.109) | data formatting | bytes 2097152

commit v5 on v4

--- a/solution.py
+++ b/solution.py
@@ -312,29 +312,38 @@
         part = wo.at[pl.ds(pl.multiple_of(at_y * size, size), size), lane_block(owner, width)]
         return remote(part, part, wos.at[at], wor.at[at], to)
 
-    def mix(b):
-        lhs = spec[b].reshape(2 * rows * cols, span)
+    def mix(b, at, size):
+        lhs = spec[b, :, :, :, :, at:at + size].reshape(2 * rows * cols, size)
         pre = lax.dot_general(
             lhs, ws[...], (((0,), (0,)), ((), ())), preferred_element_type=jnp.float32
         )
-        return (gate[b] * pre).astype(jnp.bfloat16)
-
-    def emit(b, mixed):
-        for step in range(cols // 2):
-            chip = lax.rem(lax.div(col, 2) + (2, 1, 3, 0)[step], cols // 2)
-            res = jnp.dot(
-                mixed, wo[:, lane_block(chip, 2 * width)], preferred_element_type=jnp.float32
-            ).astype(jnp.bfloat16)
-            for core in range(2):
-                osc[b, chip * 2 + core] = res[:, core * width:(core + 1) * width]
-            rest = pl.ds(pl.multiple_of(col * span, span), span)
-            targets = (far, near[0::2], near[1::2], [sib])[step]
-            for to in targets:
-                remote(
-                    osc.at[b, to], out.at[b, rest, :], oss.at[b], osr.at[b], {"col": to}
-                ).start()
-            if step == cols // 2 - 1:
-                out[b, rest, :] = osc[b, col]
+        return (gate[b, at:at + size, :] * pre).astype(jnp.bfloat16)
+
+    def emit(b, mixed, at, size, step):
+        chip = lax.rem(lax.div(col, 2) + (2, 1, 3, 0)[step], cols // 2)
+        res = jnp.dot(
+            mixed, wo[:, lane_block(chip, 2 * width)], preferred_element_type=jnp.float32
+        ).astype(jnp.bfloat16)
+        for k in range(2):
+            osc[b, chip * 2 + k, at:at + size, :] = res[:, k * width:(k + 1) * width]
+        rest = pl.ds(pl.multiple_of(col * span + at, size), size)
+        for to in (far, near[0::2], near[1::2], [sib])[step]:
+            remote(
+                osc.at[b, to, pl.ds(at, size)], out.at[b, rest, :], oss.at[b], osr.at[b],
+                {"col": to},
+            ).start()
+        if step == cols // 2 - 1:
+            out[b, rest, :] = osc[b, col, at:at + size, :]
+
+    def finish(b):
+        size = span // 2
+        low = mix(b, 0, size)
+        emit(b, low, 0, size, 0)
+        high = mix(b, size, size)
+        emit(b, high, size, size, 0)
+        mixed = jnp.concatenate([low, high], axis=0)
+        for step in range(1, cols // 2):
+            emit(b, mixed, 0, span, step)
 
     scope = jax.named_scope
     with scope("project0"):
@@ -402,10 +411,8 @@
     for b in range(batches):
         with scope("wait_second%d" % b):
             drain(ps.at[b], s2r.at[b])
-        with scope("mix%d" % b):
-            mixed = mix(b)
-        with scope("emit%d" % b):
-            emit(b, mixed)
+        with scope("finish%d" % b):
+            finish(b)
     with scope("wait_out"):
         for b in range(batches):
             drain(osc.at[b, pl.ds(0, cols - 1)], osr.at[b])

time: 48 us -> 48.1 us (level)
  no operation moved by 1% of the time
where the time goes in v5:
time: 48.1 us; the launch traced here: 48 us
  Pallas kernels  47.1 us (98%)
  local copies, waits for them, and re-layouts  0.97 us (2%)
    pallas_call x1, Pallas kernels, fused(): pl.pallas_call(functools.partial(mixer_kernel, rows, cols), out_shape=plt...  47.1 us
    unnamed x1, local copies, waits for them, and re-layouts  0.97 us

profile of v5, /device:TPU:1, one launch (start us, length us, event | category | flops | bytes accessed | tf_op | source)
XLA Modules:
  0.0 48.0 jit_solution(4690260708693547383)
XLA Ops:
  0.0 47.1 %shard_map.109 = bf16[2,2048,128]{2,1,0:T(8,128)(2,1)S(1)} custom-call(bf16[2,2048,1024]{2,1,0:T(8,128)(2,1)} %tok.1, f32[1,1024]{1,0:T(1,128)} %bitcast.3, bf16[64,1024]{1,0:T(8,128)(2,1)} %bitcast.2, bf16[1024,1024]{1,0:T(8,128)(2,1)} %wg_in.1, bf16[512,1024]{1,0:T(8,128)(2,1)} %wspec_in.1, bf16[1024,128]{1,0:T(8,128)(2,1)} %wout.1, ...), custom_call_target="tpu_custom_call" | custom-call | tf_op jit(solution)/shard_map/pallas_call | solution.py:463
  47.1 1.0 %copy.13 = bf16[2,2048,128]{2,1,0:T(8,128)(2,1)} copy(bf16[2,2048,128]{2,1,0:T(8,128)(2,1)S(1)} %shard_map.109) | data formatting | bytes 2097152

commit v6 on v4

--- a/solution.py
+++ b/solution.py
@@ -345,6 +345,11 @@
         pl.semaphore_signal(ready, inc=1, device_id={"row": to}, device_id_type=MESH)
     with scope("send0"):
         send_first(0, line)
+    for b in range(1, batches):
+        with scope("project%d" % b):
+            project(b)
+        with scope("line%d" % b):
+            send_first(b, line)
     with scope("ready"):
         pl.semaphore_wait(ready, len(turns))
     with scope("send0b"):
@@ -354,11 +359,6 @@
     share(col, 0, near[0]).start()
     share(col, 1, near[1]).start()
     share(col, 3, sib).start()
-    for b in range(1, batches):
-        with scope("project%d" % b):
-            project(b)
-        with scope("send%d" % b):
-            send_first(b, peers + [me])
     with scope("gates"):
         wg_load.wait()
         gates(0)
@@ -371,8 +371,10 @@
         f1_load.wait()
         tw_load.wait()
         f2_load.wait()
-    with scope("gates"):
-        for b in range(1, batches):
+    for b in range(1, batches):
+        with scope("send%d" % b):
+            send_first(b, aside + [me])
+        with scope("gates"):
             gates(b)
     with scope("turn"):
         quarter(far[0], y, 7, {"col": sib}).wait_recv()

time: 48 us -> 50.3 us (1.048)
  Pallas kernels: 46.9 us -> 49.3 us
    pallas_call x1, Pallas kernels: 46.9 us -> 49.3 us  [fused(): pl.pallas_call(functools.partial(mixer_kernel, rows, cols), out_shape=plt...]
where the time goes in v6:
time: 50.3 us; the launch traced here: 50.2 us
  Pallas kernels  49.3 us (98%)
  local copies, waits for them, and re-layouts  0.97 us (2%)
    pallas_call x1, Pallas kernels, fused(): pl.pallas_call(functools.partial(mixer_kernel, rows, cols), out_shape=plt...  49.3 us

profile of v6, /device:TPU:1, one launch (start us, length us, event | category | flops | bytes accessed | tf_op | source)
XLA Modules:
  0.0 50.2 jit_solution(14594545914231411007)
XLA Ops:
  0.0 49.3 %shard_map.109 = bf16[2,2048,128]{2,1,0:T(8,128)(2,1)S(1)} custom-call(bf16[2,2048,1024]{2,1,0:T(8,128)(2,1)} %tok.1, f32[1,1024]{1,0:T(1,128)} %bitcast.3, bf16[64,1024]{1,0:T(8,128)(2,1)} %bitcast.2, bf16[1024,1024]{1,0:T(8,128)(2,1)} %wg_in.1, bf16[512,1024]{1,0:T(8,128)(2,1)} %wspec_in.1, bf16[1024,128]{1,0:T(8,128)(2,1)} %wout.1, ...), custom_call_target="tpu_custom_call" | custom-call | tf_op jit(solution)/shard_map/pallas_call | solution.py:458
  49.3 1.0 %copy.13 = bf16[2,2048,128]{2,1,0:T(8,128)(2,1)} copy(bf16[2,2048,128]{2,1,0:T(8,128)(2,1)S(1)} %shard_map.109) | data formatting | bytes 2097152
